TPU v7x, 512 devices: a whole 4x4x16 slice. The times are simulated.
512 devices in a mesh: sp: 128 (over z, x, core), tp: 4 (over y).
Axes of the slice: x: 4, y: 4, z: 16, core: 2. Of those that a mesh axis runs over, the one named last changes fastest.
Arguments:
- tokens: bfloat16 [32768, 2048], P('sp'), may hold values from -6 to 6
- documents: int32 [32768], P('sp'), may hold values from 0 to 63, never falling along the last dimension, each value on 1 to 1024 neighbouring positions
- norm_gain: float32 [1, 2048], replicated, may hold values from 0.1 to 1.9
- w_query: bfloat16 [1, 2048, 2048], P(None, 'sp', 'tp'), may hold values from -0.125 to 0.125
- w_key: bfloat16 [1, 2048, 2048], P(None, 'sp', 'tp'), may hold values from -0.125 to 0.125
- w_value: bfloat16 [1, 2048, 2048], P(None, 'sp', 'tp'), may hold values from -0.125 to 0.125
- w_out: bfloat16 [1, 2048, 2048], P(None, None, 'sp'), may hold values from -0.59765625 to 0.59765625
- rel_bias: float32 [1, 32, 257], P(None, 'tp'), may hold values from -8 to 240
Outputs:
- mixed: bfloat16 [32768, 2048], P('sp')
Inputs may be any that keep to these rules, and one draw needn't show every extreme that they name: `documents`: document numbers never fall along the sequence; a document has 1 to 1024 positions.
All inputs are finite; a program needn't handle non-finite values.
Results may differ from a plain program's by a relative error of at most 0.007.
Values may be sent and summed in bfloat16 or wider, within the bound.
No kernel may reach another device: no remote copies, remote signals or barrier semaphores. Data moves between devices by JAX's collectives and lax.ppermute only.
A program may use at most 128 MiB of HBM per device.

v0:
```python
import jax
import jax.numpy as jnp
from jax import lax
from jax.sharding import Mesh
from jax.sharding import PartitionSpec as P

HEAD_DIM = 64
SEG = 64
LEFT = 4
REL_CLIP = 128
SP = ("sp_0", "sp_1", "sp_2")
EPS = 1e-06


def passed_along(x, axis, by):
    length = lax.axis_size(axis)
    pairs = [(i, i + by) for i in range(length) if 0 <= i + by < length]
    return lax.ppermute(x, axis, pairs)


def in_one_piece(arrays, axis, dim, along):
    ends, at = ([], 0)
    for a in arrays[:-1]:
        at += a.shape[along]
        ends.append(at)
    both = jnp.concatenate(arrays, axis=along)
    return tuple(jnp.split(lax.all_gather(both, axis, axis=dim, tiled=True), ends, axis=along))


def laid_out(pieces, dim):
    shape = list(pieces.shape[1:])
    shape[dim] *= pieces.shape[0]
    return jnp.moveaxis(pieces, 0, dim).reshape(shape)


def from_everyone(x, axis):
    length = lax.axis_size(axis)
    return lax.all_to_all(jnp.broadcast_to(x[None], (length, *x.shape)), axis, 0, 0, tiled=True)


def collect(x, axis, dim):
    return laid_out(from_everyone(x, axis), dim)


def gather_in_order(x, axes, order):
    pieces = x[None]
    for k in order:
        pieces = lax.all_gather(pieces, axes[k], axis=0, tiled=True)
    held = [lax.axis_size(axes[k]) for k in reversed(order)]
    pieces = pieces.reshape(*held, *x.shape)
    turned = sorted(range(len(order)), key=lambda place: order[len(order) - 1 - place])
    return pieces.transpose(*turned, *range(len(order), pieces.ndim)).reshape(-1, *x.shape)


def gather_axes(x, axes, order, dim):
    return laid_out(gather_in_order(x, axes, order), dim)


def banded_bias(bias_table, query_rows, key_rows, reach_rows):
    span_len = query_rows + key_rows - 1
    steps_back = jnp.arange(span_len, dtype=jnp.int32) - (key_rows - 1) + reach_rows
    lookup = jnp.clip(steps_back, -REL_CLIP, REL_CLIP) + REL_CLIP
    bias_line = jnp.take(bias_table, lookup, axis=1)
    reversed_line = bias_line[:, ::-1]
    repeated = jnp.tile(reversed_line, (1, query_rows))
    skewed = repeated[:, query_rows - 1 : query_rows - 1 + query_rows * (span_len - 1)]
    skewed = skewed.reshape(bias_table.shape[0], query_rows, span_len - 1)
    return skewed[:, :, :key_rows]


def attend(queries, keys_all, values_all, query_pos, key_pos, query_doc, key_doc, bias_table):
    query_rows = queries.shape[0]
    key_rows = keys_all.shape[0]
    reach_rows = key_rows - query_rows
    scores = jnp.einsum(
        "qhe,khe->hqk", queries, keys_all, preferred_element_type=jnp.float32
    ) * HEAD_DIM ** (-0.5)
    scores = scores + banded_bias(bias_table, query_rows, key_rows, reach_rows)
    query_seg = query_pos // SEG
    key_seg = key_pos // SEG
    allowed = (
        (key_pos[None, :] >= 0)
        & (key_seg[None, :] <= query_seg[:, None])
        & (key_seg[None, :] >= query_seg[:, None] - LEFT)
        & (key_doc[None, :] == query_doc[:, None])
    )
    scores = jnp.where(allowed[None], scores, -1e30)
    peak = jnp.max(scores, axis=-1, keepdims=True)
    raised = jnp.exp(scores - peak)
    weights_bf = (raised / jnp.sum(raised, axis=-1, keepdims=True)).astype(jnp.bfloat16)
    return jnp.einsum(
        "hqk,khe->qhe", weights_bf, values_all, preferred_element_type=jnp.float32
    ).astype(jnp.bfloat16)


def body(tokens, documents, norm_gain, w_query, w_key, w_value, w_out, rel_bias):
    local_rows = tokens.shape[0]
    reach_rows = LEFT * SEG
    width_local = w_query.shape[2]
    heads_local = width_local // HEAD_DIM
    offset = lax.axis_index(SP) * local_rows
    query_pos = offset + jnp.arange(local_rows, dtype=jnp.int32)
    key_pos = offset - reach_rows + jnp.arange(reach_rows + local_rows, dtype=jnp.int32)
    widened = tokens.astype(jnp.float32)
    normed = (
        widened
        * lax.rsqrt(jnp.mean(widened * widened, axis=-1, keepdims=True) + EPS)
        * norm_gain[0]
    ).astype(jnp.bfloat16)
    before, prior_docs = passed_along((normed, documents), SP, 1)
    extended = jnp.concatenate([before, normed], axis=0)
    pieces = in_one_piece((w_query[0], w_key[0], w_value[0]), SP, 0, 1)
    query_sum = jnp.dot(normed, pieces[0], preferred_element_type=jnp.float32)
    key_sum = jnp.dot(extended, pieces[1], preferred_element_type=jnp.float32)
    value_sum = jnp.dot(extended, pieces[2], preferred_element_type=jnp.float32)
    queries = query_sum.astype(jnp.bfloat16)
    keys_all = key_sum.astype(jnp.bfloat16)
    values_all = value_sum.astype(jnp.bfloat16)
    key_doc = jnp.concatenate([prior_docs, documents], axis=0)
    attended = attend(
        queries.reshape(local_rows, heads_local, HEAD_DIM),
        keys_all.reshape(reach_rows + local_rows, heads_local, HEAD_DIM),
        values_all.reshape(reach_rows + local_rows, heads_local, HEAD_DIM),
        query_pos,
        key_pos,
        documents,
        key_doc,
        rel_bias[0],
    ).reshape(local_rows, width_local)
    all_heads = collect(attended, "tp", 1)
    return (
        widened
        + jnp.dot(
            all_heads, gather_axes(w_out[0], SP, (1, 0, 2), 1), preferred_element_type=jnp.float32
        )
    ).astype(jnp.bfloat16)


def solution(mesh):
    split = Mesh(mesh.devices.reshape(16, 4, 2, mesh.shape["tp"]), ("sp_0", "sp_1", "sp_2", "tp"))
    placed = (
        P(SP, None),
        P(SP),
        P(),
        P(None, SP, "tp"),
        P(None, SP, "tp"),
        P(None, SP, "tp"),
        P(None, None, SP),
        P(None, "tp", None),
    )
    return jax.shard_map(body, mesh=split, in_specs=placed, out_specs=P(SP, None), check_vma=False)
```

profile of v0, /device:TPU:32, one launch (start us, length us, event | category | flops | bytes accessed | tf_op | source)
XLA Modules:
  0.0 303.6 jit_solution(17535925062422447760)
XLA Ops:
  6.5 0.0 copy-start.1
  6.5 0.0 copy-start.3
  6.5 0.0 copy-start.4
  6.5 0.0 copy-start.2
  6.5 0.0 all-gather.6.cloned.1.call-start
  6.6 14.3 %all_gather.13 = bf16[4,2048,16]{1,2,0:T(8,128)(2,1)} all-gather(bf16[1,2048,16]{1,2,0:T(8,128)(2,1)} %param.14), channel_id=1, replica_groups=mesh['sp_0'=16,'sp_1'=4,'sp_2'=2,'tp'=4] {'sp_1'}, dimensions={0}, use_global_device_ids=true | all-gather | bytes 327680 | tf_op jit(solution)/shard_map/all_gather | solution.py:48
  20.9 0.0 all-gather.6.cloned.1.call-update
  21.0 0.0 all-gather.4.cloned.1.call-start
  21.0 1.4 pad_maximum_fusion.7
  22.4 0.0 all-gather.4.cloned.1.call-update
  22.4 0.0 all-gather.8.cloned.1.call-start
  22.4 79.5 %all-gather.6.cloned.1.call-done = bf16[64,2048,16]{1,2,0:T(8,128)(2,1)} async-done(((bf16[4,2048,16]{1,2,0:T(8,128)(2,1)}), bf16[64,2048,16]{1,2,0:T(8,128)(2,1)}) %all-gather.6.cloned.1.call-update) | async-done | bytes 4194320 | tf_op jit(solution)/shard_map/all_gather | solution.py:48
  101.9 0.0 all-gather.8.cloned.1.call-update
  101.9 0.0 copy-done.1
  102.0 0.3 fusion.3
  102.2 0.0 copy-done.3
  102.3 1.3 fusion.5
  103.5 1.9 collective-permute-start
  105.5 0.0 copy-done.4
  105.5 3.5 %collective-permute-start.1 = (s32[256]{0:T(256)S(1)}, s32[256]{0:T(256)S(1)}, u32[]{:S(2)}, u32[]{:S(2)}) collective-permute-start(s32[256]{0:T(256)S(1)} %copy-done.4), channel_id=1, source_target_pairs={{0,4},{4,8},{8,12},{12,16},{16,20},{20,24},{24,28},{28,32},{32,36}... | collective-permute-start | bytes 3080 | tf_op jit(solution)/shard_map/ppermute | solution.py:18
  109.1 0.0 copy-done.2
  109.1 0.1 copy.21
  109.2 1.6 gather_fusion
  110.8 0.2 select_bitcast_fusion
  111.0 0.5 rev.3
  111.4 0.1 copy.22
  111.6 3.2 %tile.4 = f32[8,256,767]{2,1,0:T(8,128)} broadcast(f32[8,767]{1,0:T(8,128)S(1)} %copy.22), dimensions={0,2} | broadcast | bytes 6307808 | tf_op jit(solution)/shard_map/tile | solution.py:65
  114.7 8.8 %tile.10 = f32[8,196352]{1,0:T(8,128)} reshape(f32[8,256,767]{2,1,0:T(8,128)} %tile.4) | data formatting | bytes 12566528 | tf_op jit(solution)/shard_map/tile | solution.py:65
  123.5 5.5 %slice.10 = f32[8,196096]{1,0:T(8,128)} slice(f32[8,196352]{1,0:T(8,128)} %tile.10), slice={[0:8], [255:196351]} | slice | bytes 12550144 | tf_op jit(solution)/shard_map/slice | solution.py:66
  128.9 12.4 %reshape.213 = f32[8,256,766]{2,1,0:T(8,128)} reshape(f32[8,196096]{1,0:T(8,128)} %slice.10) | data formatting | bytes 12550144 | tf_op jit(solution)/shard_map/reshape | solution.py:67
  141.3 0.0 collective-permute-done.1
  141.3 0.3 compare_and_fusion
  141.6 104.4 %all-gather.4.cloned.1.call-done = bf16[2048,1536]{1,0:T(8,128)(2,1)} async-done(((bf16[16,1536]{1,0:T(8,128)(2,1)}), bf16[2048,1536]{1,0:T(8,128)(2,1)}) %all-gather.4.cloned.1.call-update) | async-done | bytes 6291472 | tf_op jit(solution)/shard_map/all_gather | solution.py:27
  246.0 0.0 slice-start
  246.0 3.5 %fusion.20 = bf16[256,512]{1,0:T(8,128)(2,1)} fusion(bf16[256,2048]{1,0:T(8,128)(2,1)} %fusion.5, bf16[2048,1536]{1,0:T(8,128)(2,1)} %all-gather.4.cloned.1.call-done), kind=kOutput, calls=%fused_computation.24 | convolution fusion | flops 537001984 | bytes 3407872 | tf_op jit(solution)/shard_map/dot_general | solution.py:113
  249.5 1.1 copy.20
  250.6 0.0 slice-start.1
  250.6 0.0 collective-permute-done
  250.6 3.7 %fusion.16 = bf16[512,512]{0,1:T(8,128)(2,1)S(1)} fusion(bf16[2048,1536]{1,0:T(8,128)(2,1)} %all-gather.4.cloned.1.call-done, bf16[256,2048]{1,0:T(8,128)(2,1)} %fusion.5, bf16[256,2048]{1,0:T(8,128)(2,1)} %collective-permute-done), kind=kOutput, calls=%fused_computation.22 | convolution fusion | flops 1078198272 | bytes 4718592 | tf_op jit(solution)/shard_map/dot_general | solution.py:114
  254.3 0.0 slice-done
  254.3 0.0 slice-done.1
  254.3 0.9 fusion.1
  255.2 0.0 copy-start
  255.2 1.7 fusion.34
  257.0 3.6 %fusion.13 = bf16[512,512]{0,1:T(8,128)(2,1)S(1)} fusion(bf16[2048,1536]{1,0:T(8,128)(2,1)} %all-gather.4.cloned.1.call-done, bf16[256,2048]{1,0:T(8,128)(2,1)} %fusion.5, bf16[256,2048]{1,0:T(8,128)(2,1)} %collective-permute-done), kind=kOutput, calls=%fused_computation.21 | convolution fusion | flops 1078198272 | bytes 4718592 | tf_op jit(solution)/shard_map/dot_general | solution.py:115
  260.6 0.0 copy-done
  260.6 8.9 %fusion.19 = bf16[8,64,256]{2,1,0:T(8,128)(2,1)S(1)} fusion(bf16[512,8,64]{0,2,1:T(8,128)(2,1)S(1)} %bitcast.45, f32[8,256]{1,0:T(8,128)S(1)} %fusion.34, f32[8,256,512]{2,1,0:T(8,128)} %copy-done), kind=kOutput, calls=%fused_computation.23 | convolution fusion | flops 137497088 | bytes 4988928 | tf_op jit(solution)/shard_map/hqk,khe->qhe/dot_general | solution.py:91
  269.5 1.0 broadcast_in_dim.45
  270.5 4.3 %all-to-all-start = ((bf16[4,256,512]{1,2,0:T(8,128)(2,1)}), bf16[4,256,512]{1,2,0:T(8,128)(2,1)S(1)}, u32[]{:S(2)}, u32[]{:S(2)}) async-start(bf16[4,256,512]{1,2,0:T(8,128)(2,1)} %broadcast_in_dim.45), calls=%async_computation | async-start | bytes 2097152 | tf_op jit(solution)/shard_map/all_to_all | solution.py:38
  274.8 0.0 all-gather.8.cloned.1.call-done
  274.8 8.2 %copy.23 = bf16[16,4,2,2048,16]{3,4,2,1,0:T(8,128)(2,1)} copy(bf16[16,4,2,2048,16]{3,4,1,0,2:T(8,128)(2,1)} %bitcast.34) | data formatting | bytes 16777216 | tf_op jit(solution)/shard_map/transpose | solution.py:52
  283.1 7.3 %all-to-all-done = bf16[4,256,512]{1,2,0:T(8,128)(2,1)S(1)} async-done(((bf16[4,256,512]{1,2,0:T(8,128)(2,1)}), bf16[4,256,512]{1,2,0:T(8,128)(2,1)S(1)}, u32[]{:S(2)}, u32[]{:S(2)}) %all-to-all-start) | async-done | bytes 1048608 | tf_op jit(solution)/shard_map/all_to_all | solution.py:38
  290.4 6.7 %fusion.2 = bf16[256,2048]{1,0:T(8,128)(2,1)} fusion(bf16[256,2048]{0,1:T(8,128)(2,1)S(1)} %bitcast.37, bf16[2048,2048]{0,1:T(8,128)(2,1)} %bitcast.35, bf16[256,2048]{1,0:T(8,128)(2,1)S(1)} %copy-done.1), kind=kOutput, calls=%fused_computation.9 | convolution fusion | flops 2149056512 | bytes 11534336 | tf_op jit(solution)/shard_map/dot_general | solution.py:133
  (9 shorter events, 0.1 us)
Async XLA Ops:
  6.5 95.4 %copy-start.1 = (bf16[256,2048]{1,0:T(8,128)(2,1)S(1)}, bf16[256,2048]{1,0:T(8,128)(2,1)}, u32[]{:S(2)}) copy-start(bf16[256,2048]{1,0:T(8,128)(2,1)} %param.8) | copy-start | bytes 3145732
  6.5 95.7 %copy-start.3 = (f32[1,2048]{1,0:T(1,128)S(1)}, f32[1,2048]{1,0:T(1,128)}, u32[]{:S(2)}) copy-start(f32[1,2048]{1,0:T(1,128)} %param.10) | copy-start | bytes 24580
  6.5 98.9 %copy-start.4 = (s32[256]{0:T(256)S(1)}, s32[256]{0:T(256)}, u32[]{:S(2)}) copy-start(s32[256]{0:T(256)} %param.9) | copy-start | bytes 3076
  6.5 102.5 %copy-start.2 = (f32[1,8,257]{2,1,0:T(8,128)S(1)}, f32[1,8,257]{2,1,0:T(8,128)}, u32[]{:S(2)}) copy-start(f32[1,8,257]{2,1,0:T(8,128)} %param.15) | copy-start | bytes 24676
  6.5 95.4 %all-gather.6.cloned.1.call-start = ((), (), s32[]{:S(2)}) async-start(), calls=%async_computation.2 | async-start | bytes 4456448 | tf_op jit(solution)/shard_map/all_gather | solution.py:48
  21.0 225.1 %all-gather.4.cloned.1.call-start = ((), (), s32[]{:S(2)}) async-start(), calls=%async_computation.1 | async-start | bytes 6340608 | tf_op jit(solution)/shard_map/all_gather | solution.py:27
  22.4 252.4 %all-gather.8.cloned.1.call-start = ((), (), s32[]{:S(2)}) async-start(), calls=%async_computation.3 | async-start | bytes 12582912 | tf_op jit(solution)/shard_map/all_gather | solution.py:48
  103.5 147.0 %collective-permute-start = (bf16[256,2048]{1,0:T(8,128)(2,1)}, bf16[256,2048]{1,0:T(8,128)(2,1)}, u32[]{:S(2)}, u32[]{:S(2)}) collective-permute-start(bf16[256,2048]{1,0:T(8,128)(2,1)} %fusion.5), channel_id=1, source_target_pairs={{0,4},{4,8},{8,12},{12,16},{16,20},{20,24},{24,28},{28,32},{32,36}... | collective-permute-start | bytes 3145736 | tf_op jit(solution)/shard_map/ppermute | solution.py:18
  105.5 35.9 %collective-permute-start.1 = (s32[256]{0:T(256)S(1)}, s32[256]{0:T(256)S(1)}, u32[]{:S(2)}, u32[]{:S(2)}) collective-permute-start(s32[256]{0:T(256)S(1)} %copy-done.4), channel_id=1, source_target_pairs={{0,4},{4,8},{8,12},{12,16},{16,20},{20,24},{24,28},{28,32},{32,36}... | collective-permute-start | bytes 3080 | tf_op jit(solution)/shard_map/ppermute | solution.py:18
  246.0 8.2 %slice-start = ((s8[6291456]{0:T(1024)(128)(4,1)}), s8[2097152]{0:T(1024)(128)(4,1)S(1)}, s32[]{:S(2)}) async-start(s8[6291456]{0:T(1024)(128)(4,1)} %bitcast.32), calls=%async_computation.4 | async-start | bytes 4194304
  250.6 3.7 %slice-start.1 = ((s8[6291456]{0:T(1024)(128)(4,1)}), s8[4194304]{0:T(1024)(128)(4,1)S(1)}, s32[]{:S(2)}) async-start(s8[6291456]{0:T(1024)(128)(4,1)} %bitcast.32), calls=%async_computation.5 | async-start | bytes 8388608
  255.2 5.4 %copy-start = (f32[8,256,512]{2,1,0:T(8,128)}, f32[8,256,512]{2,1,0:T(8,128)S(1)}, u32[]{:S(2)}) copy-start(f32[8,256,512]{2,1,0:T(8,128)S(1)} %fusion.1) | copy-start | bytes 12582916
  270.5 19.9 %all-to-all-start = ((bf16[4,256,512]{1,2,0:T(8,128)(2,1)}), bf16[4,256,512]{1,2,0:T(8,128)(2,1)S(1)}, u32[]{:S(2)}, u32[]{:S(2)}) async-start(bf16[4,256,512]{1,2,0:T(8,128)(2,1)} %broadcast_in_dim.45), calls=%async_computation | async-start | bytes 2097152 | tf_op jit(solution)/shard_map/all_to_all | solution.py:38
Sparse Core Ops, SparseCore 0:
  21.1 80.7 all-gather.5
  105.0 140.9 all-gather.3
  248.1 24.9 all-gather.7
where the time goes:
time: 304 us
  waiting for transfers between devices  191 us (63%)
  local copies, waits for them, and re-layouts  42.4 us (14%)
  matrix products  27.3 us (9%)
  blocking collectives  14.3 us (5%)
  between operations  13.4 us (4%)
  starting transfers between devices  9.79 us (3%)
  other arithmetic  5.19 us (2%)
    all_gather x1, waiting for transfers between devices, in_one_piece(): lax.all_gather(both, axis, axis=dim, tiled=True)  104 us
    all_gather x2, waiting for transfers between devices, gather_in_order(): pieces = lax.all_gather(pieces, axes[k], axis=0, tiled=True)  79.5 us
    all_gather x1, blocking collectives, gather_in_order(): pieces = lax.all_gather(pieces, axes[k], axis=0, tiled=True)  14.3 us
    reshape x1, local copies, waits for them, and re-layouts, banded_bias(): skewed = skewed.reshape(bias_table.shape[0], query_rows, span_len - 1)  12.4 us
    another operation x2, local copies, waits for them, and re-layouts, banded_bias(): repeated = jnp.tile(reversed_line, (1, query_rows))  11.9 us
    dot_general x1, matrix products, attend(): jnp.einsum('hqk,khe->qhe', weights_bf, values_all, preferred_element_type...  8.9 us
    transpose x1, local copies, waits for them, and re-layouts, gather_in_order(): pieces.transpose(*turned, *range(len(order), pieces.ndim))  8.25 us
    all_to_all x1, waiting for transfers between devices, from_everyone(): lax.all_to_all(jnp.broadcast_to(x[None], (length, *x.shape)), axis, 0, 0,...  7.32 us
  transfers between devices with their start and end apart: 6, of which 3 were waited for; matrix products, arithmetic and copies ran while one was open for 22% of the time, Pallas kernels for 0%

commit v1 on v0

--- a/solution.py
+++ b/solution.py
@@ -10,6 +10,13 @@
 REL_CLIP = 128
 SP = ("sp_0", "sp_1", "sp_2")
 EPS = 1e-06
+
+
+def swapped_in(value, axis, dim):
+    n_dev = lax.axis_size(axis)
+    parts = jnp.stack([value for _ in range(n_dev)])
+    parts = lax.all_to_all(parts, axis, split_axis=0, concat_axis=0)
+    return jnp.concatenate(parts, axis=dim)
 
 
 def passed_along(x, axis, by):
@@ -45,7 +52,7 @@
 def gather_in_order(x, axes, order):
     pieces = x[None]
     for k in order:
-        pieces = lax.all_gather(pieces, axes[k], axis=0, tiled=True)
+        pieces = swapped_in(pieces, axes[k], 0)
     held = [lax.axis_size(axes[k]) for k in reversed(order)]
     pieces = pieces.reshape(*held, *x.shape)
     turned = sorted(range(len(order)), key=lambda place: order[len(order) - 1 - place])

time: 304 us -> 331 us (1.089)
  the two profiles are of different devices: /device:TPU:32 before, /device:TPU:1 now
where the time goes in v1:
time: 331 us; the launch traced here: 330 us
  waiting for transfers between devices  179 us (54%)
  local copies, waits for them, and re-layouts  45.7 us (14%)
  blocking collectives  28.6 us (9%)
  starting transfers between devices  25.8 us (8%)
  matrix products  25.8 us (8%)
  between operations  13.7 us (4%)
  other arithmetic  11.9 us (4%)
    all_gather x1, waiting for transfers between devices, in_one_piece(): lax.all_gather(both, axis, axis=dim, tiled=True)  172 us
    all_to_all x2, blocking collectives, swapped_in(): parts = lax.all_to_all(parts, axis, split_axis=0, concat_axis=0)  28.6 us
    all_to_all x1, starting transfers between devices, swapped_in(): parts = lax.all_to_all(parts, axis, split_axis=0, concat_axis=0)  15.1 us
    reshape x1, local copies, waits for them, and re-layouts, banded_bias(): skewed = skewed.reshape(bias_table.shape[0], query_rows, span_len - 1)  12.3 us
    another operation x2, local copies, waits for them, and re-layouts, banded_bias(): repeated = jnp.tile(reversed_line, (1, query_rows))  11.9 us
    all_to_all x1, local copies, waits for them, and re-layouts, swapped_in(): parts = lax.all_to_all(parts, axis, split_axis=0, concat_axis=0)  8.28 us
    another operation x1, other arithmetic, swapped_in(): parts = jnp.stack([value for _ in range(n_dev)])  7.49 us
    dot_general x1, matrix products, attend(): jnp.einsum('hqk,khe->qhe', weights_bf, values_all, preferred_element_type...  7.45 us
  transfers between devices with their start and end apart: 5, of which 2 were waited for; matrix products, arithmetic and copies ran while one was open for 20% of the time, Pallas kernels for 0%

profile of v1, /device:TPU:1, one launch (start us, length us, event | category | flops | bytes accessed | tf_op | source)
XLA Modules:
  0.0 330.3 jit_solution(7637656796647401429)
XLA Ops:
  6.5 0.9 stack.9
  7.4 10.2 %all_to_all.20 = bf16[4,1,2048,16]{2,3,1,0:T(8,128)(2,1)S(1)} all-to-all(bf16[4,1,2048,16]{2,3,1,0:T(8,128)(2,1)S(1)} %stack.9), channel_id=1, replica_groups=mesh['sp_0'=16,'sp_1'=4,'sp_2'=2,'tp'=4] {'sp_1'}, dimensions={0} | all-to-all | bytes 524288 | tf_op jit(solution)/shard_map/all_to_all | solution.py:18
  17.6 2.5 stack.10
  20.1 0.0 copy-start.2
  20.1 0.0 copy-start.3
  20.1 0.0 copy-start.4
  20.1 0.0 copy-start.1
  20.1 0.0 copy-start.6
  20.1 0.0 copy-start.7
  20.1 0.0 copy-start.5
  20.1 15.1 %all-to-all-start.2 = ((bf16[16,4,2048,16]{2,3,1,0:T(8,128)(2,1)}), bf16[16,4,2048,16]{2,3,1,0:T(8,128)(2,1)}, u32[]{:S(2)}, u32[]{:S(2)}) async-start(bf16[16,4,2048,16]{2,3,1,0:T(8,128)(2,1)} %stack.10), calls=%async_computation.2 | async-start | bytes 8388608 | tf_op jit(solution)/shard_map/all_to_all | solution.py:18
  35.3 0.0 all-gather.2.cloned.1.call-start
  35.3 0.0 copy-done.2
  35.3 0.0 copy-done.3
  35.3 0.0 copy-done.4
  35.3 0.6 pad_maximum_fusion.8
  36.0 0.0 all-gather.2.cloned.1.call-update
  36.0 0.0 copy-done.1
  36.0 0.3 fusion.3
  36.3 0.0 copy-done.6
  36.3 1.3 fusion.5
  37.6 4.4 %collective-permute-start = (bf16[256,2048]{1,0:T(8,128)(2,1)}, bf16[256,2048]{1,0:T(8,128)(2,1)}, u32[]{:S(2)}, u32[]{:S(2)}) collective-permute-start(bf16[256,2048]{1,0:T(8,128)(2,1)} %fusion.5), channel_id=1, source_target_pairs={{0,4},{4,8},{8,12},{12,16},{16,20},{20,24},{24,28},{28,32},{32,36}... | collective-permute-start | bytes 3145736 | tf_op jit(solution)/shard_map/ppermute | solution.py:25
  42.0 0.0 copy-done.7
  42.0 1.9 collective-permute-start.1
  44.1 0.0 copy-done.5
  44.1 0.1 copy.18
  44.2 1.6 gather_fusion
  45.8 0.2 select_bitcast_fusion
  46.0 0.5 rev.3
  46.4 0.1 copy.19
  46.6 3.2 tile.4
  49.7 8.7 %tile.10 = f32[8,196352]{1,0:T(8,128)} reshape(f32[8,256,767]{2,1,0:T(8,128)} %tile.4) | data formatting | bytes 12566528 | tf_op jit(solution)/shard_map/tile | solution.py:72
  58.4 5.5 %slice.10 = f32[8,196096]{1,0:T(8,128)} slice(f32[8,196352]{1,0:T(8,128)} %tile.10), slice={[0:8], [255:196351]} | slice | bytes 12550144 | tf_op jit(solution)/shard_map/slice | solution.py:73
  63.9 12.3 %reshape.215 = f32[8,256,766]{2,1,0:T(8,128)} reshape(f32[8,196096]{1,0:T(8,128)} %slice.10) | data formatting | bytes 12550144 | tf_op jit(solution)/shard_map/reshape | solution.py:74
  76.2 0.0 collective-permute-done.1
  76.2 0.3 compare_and_fusion
  76.4 172.5 %all-gather.2.cloned.1.call-done = bf16[2048,1536]{1,0:T(8,128)(2,1)} async-done(((bf16[16,1536]{1,0:T(8,128)(2,1)}), bf16[2048,1536]{1,0:T(8,128)(2,1)}) %all-gather.2.cloned.1.call-update) | async-done | bytes 6291472 | tf_op jit(solution)/shard_map/all_gather | solution.py:34
  248.9 0.0 slice-start
  248.9 3.5 %fusion.20 = bf16[256,512]{1,0:T(8,128)(2,1)} fusion(bf16[256,2048]{1,0:T(8,128)(2,1)} %fusion.5, bf16[2048,1536]{1,0:T(8,128)(2,1)} %all-gather.2.cloned.1.call-done), kind=kOutput, calls=%fused_computation.25 | convolution fusion | flops 537001984 | bytes 3407872 | tf_op jit(solution)/shard_map/dot_general | solution.py:120
  252.4 1.1 copy.17
  253.5 0.0 slice-start.1
  253.5 0.0 collective-permute-done
  253.5 3.7 %fusion.16 = bf16[512,512]{0,1:T(8,128)(2,1)S(1)} fusion(bf16[2048,1536]{1,0:T(8,128)(2,1)} %all-gather.2.cloned.1.call-done, bf16[256,2048]{1,0:T(8,128)(2,1)} %fusion.5, bf16[256,2048]{1,0:T(8,128)(2,1)} %collective-permute-done), kind=kOutput, calls=%fused_computation.23 | convolution fusion | flops 1078198272 | bytes 4718592 | tf_op jit(solution)/shard_map/dot_general | solution.py:121
  257.2 0.0 slice-done
  257.2 0.0 slice-done.1
  257.2 0.9 fusion.1
  258.2 0.0 copy-start
  258.2 1.7 fusion.34
  259.9 3.5 %fusion.13 = bf16[512,512]{0,1:T(8,128)(2,1)S(1)} fusion(bf16[2048,1536]{1,0:T(8,128)(2,1)} %all-gather.2.cloned.1.call-done, bf16[256,2048]{1,0:T(8,128)(2,1)} %fusion.5, bf16[256,2048]{1,0:T(8,128)(2,1)} %collective-permute-done), kind=kOutput, calls=%fused_computation.22 | convolution fusion | flops 1078198272 | bytes 4718592 | tf_op jit(solution)/shard_map/dot_general | solution.py:122
  263.4 0.0 copy-done
  263.5 7.5 %fusion.19 = bf16[8,64,256]{2,1,0:T(8,128)(2,1)S(1)} fusion(bf16[512,8,64]{0,2,1:T(8,128)(2,1)S(1)} %bitcast.50, f32[8,256]{1,0:T(8,128)S(1)} %fusion.34, f32[8,256,512]{2,1,0:T(8,128)} %copy-done), kind=kOutput, calls=%fused_computation.24 | convolution fusion | flops 137497088 | bytes 4988928 | tf_op jit(solution)/shard_map/hqk,khe->qhe/dot_general | solution.py:98
  270.9 0.0 all-to-all-done.2
  270.9 7.5 %pad_maximum_fusion = bf16[2,64,2048,16]{2,3,1,0:T(8,128)(2,1)} fusion(bf16[1,64,2048,16]{2,3,1,0:T(8,128)(2,1)} %bitcast.15), kind=kLoop, calls=%fused_computation.2 | loop fusion | flops 4194304 | bytes 12582912 | tf_op jit(solution)/shard_map/stack | solution.py:17
  278.4 18.4 %all_to_all.21 = bf16[2,64,2048,16]{2,3,1,0:T(8,128)(2,1)} all-to-all(bf16[2,64,2048,16]{2,3,1,0:T(8,128)(2,1)} %pad_maximum_fusion), channel_id=1, replica_groups=mesh['sp_0'=16,'sp_1'=4,'sp_2'=2,'tp'=4] {'sp_2'}, dimensions={0} | all-to-all | bytes 16777216 | tf_op jit(solution)/shard_map/all_to_all | solution.py:18
  296.8 1.0 broadcast_in_dim.45
  297.9 4.3 %all-to-all-start = ((bf16[4,256,512]{1,2,0:T(8,128)(2,1)}), bf16[4,256,512]{1,2,0:T(8,128)(2,1)S(1)}, u32[]{:S(2)}, u32[]{:S(2)}) async-start(bf16[4,256,512]{1,2,0:T(8,128)(2,1)} %broadcast_in_dim.45), calls=%async_computation | async-start | bytes 2097152 | tf_op jit(solution)/shard_map/all_to_all | solution.py:45
  302.1 8.3 %copy.20 = bf16[2,64,2048,16]{2,3,0,1:T(8,128)(2,1)} copy(bf16[2,64,2048,16]{2,3,1,0:T(8,128)(2,1)} %all_to_all.21) | data formatting | bytes 16777216 | tf_op jit(solution)/shard_map/all_to_all | solution.py:18
  310.4 6.3 %all-to-all-done = bf16[4,256,512]{1,2,0:T(8,128)(2,1)S(1)} async-done(((bf16[4,256,512]{1,2,0:T(8,128)(2,1)}), bf16[4,256,512]{1,2,0:T(8,128)(2,1)S(1)}, u32[]{:S(2)}, u32[]{:S(2)}) %all-to-all-start) | async-done | bytes 1048608 | tf_op jit(solution)/shard_map/all_to_all | solution.py:45
  316.7 6.7 %fusion.2 = bf16[256,2048]{1,0:T(8,128)(2,1)} fusion(bf16[256,2048]{0,1:T(8,128)(2,1)S(1)} %bitcast.41, bf16[2048,2048]{0,1:T(8,128)(2,1)} %bitcast.38, bf16[256,2048]{1,0:T(8,128)(2,1)S(1)} %copy-done.1), kind=kOutput, calls=%fused_computation.10 | convolution fusion | flops 2149056512 | bytes 11534336 | tf_op jit(solution)/shard_map/dot_general | solution.py:140
  (9 shorter events, 0.1 us)
Async XLA Ops:
  20.1 15.2 %copy-start.2 = (bf16[1,16,512]{2,1,0:T(8,128)(2,1)S(1)}, bf16[1,16,512]{2,1,0:T(8,128)(2,1)}, u32[]{:S(2)}) copy-start(bf16[1,16,512]{2,1,0:T(8,128)(2,1)} %param.13) | copy-start | bytes 49156
  20.1 15.3 %copy-start.3 = (bf16[1,16,512]{2,1,0:T(8,128)(2,1)S(1)}, bf16[1,16,512]{2,1,0:T(8,128)(2,1)}, u32[]{:S(2)}) copy-start(bf16[1,16,512]{2,1,0:T(8,128)(2,1)} %param.12) | copy-start | bytes 49156
  20.1 15.3 %copy-start.4 = (bf16[1,16,512]{2,1,0:T(8,128)(2,1)S(1)}, bf16[1,16,512]{2,1,0:T(8,128)(2,1)}, u32[]{:S(2)}) copy-start(bf16[1,16,512]{2,1,0:T(8,128)(2,1)} %param.11) | copy-start | bytes 49156
  20.1 15.9 %copy-start.1 = (bf16[256,2048]{1,0:T(8,128)(2,1)S(1)}, bf16[256,2048]{1,0:T(8,128)(2,1)}, u32[]{:S(2)}) copy-start(bf16[256,2048]{1,0:T(8,128)(2,1)} %param.8) | copy-start | bytes 3145732
  20.1 16.2 %copy-start.6 = (f32[1,2048]{1,0:T(1,128)S(1)}, f32[1,2048]{1,0:T(1,128)}, u32[]{:S(2)}) copy-start(f32[1,2048]{1,0:T(1,128)} %param.10) | copy-start | bytes 24580
  20.1 21.9 %copy-start.7 = (s32[256]{0:T(256)S(1)}, s32[256]{0:T(256)}, u32[]{:S(2)}) copy-start(s32[256]{0:T(256)} %param.9) | copy-start | bytes 3076
  20.1 24.0 %copy-start.5 = (f32[1,8,257]{2,1,0:T(8,128)S(1)}, f32[1,8,257]{2,1,0:T(8,128)}, u32[]{:S(2)}) copy-start(f32[1,8,257]{2,1,0:T(8,128)} %param.15) | copy-start | bytes 24676
  20.1 250.8 %all-to-all-start.2 = ((bf16[16,4,2048,16]{2,3,1,0:T(8,128)(2,1)}), bf16[16,4,2048,16]{2,3,1,0:T(8,128)(2,1)}, u32[]{:S(2)}, u32[]{:S(2)}) async-start(bf16[16,4,2048,16]{2,3,1,0:T(8,128)(2,1)} %stack.10), calls=%async_computation.2 | async-start | bytes 8388608 | tf_op jit(solution)/shard_map/all_to_all | solution.py:18
  35.3 213.7 %all-gather.2.cloned.1.call-start = ((), (), s32[]{:S(2)}) async-start(), calls=%async_computation.4 | async-start | bytes 6340608 | tf_op jit(solution)/shard_map/all_gather | solution.py:34
  37.6 215.9 %collective-permute-start = (bf16[256,2048]{1,0:T(8,128)(2,1)}, bf16[256,2048]{1,0:T(8,128)(2,1)}, u32[]{:S(2)}, u32[]{:S(2)}) collective-permute-start(bf16[256,2048]{1,0:T(8,128)(2,1)} %fusion.5), channel_id=1, source_target_pairs={{0,4},{4,8},{8,12},{12,16},{16,20},{20,24},{24,28},{28,32},{32,36}... | collective-permute-start | bytes 3145736 | tf_op jit(solution)/shard_map/ppermute | solution.py:25
  42.0 34.1 %collective-permute-start.1 = (s32[256]{0:T(256)S(1)}, s32[256]{0:T(256)S(1)}, u32[]{:S(2)}, u32[]{:S(2)}) collective-permute-start(s32[256]{0:T(256)S(1)} %copy-done.7), channel_id=1, source_target_pairs={{0,4},{4,8},{8,12},{12,16},{16,20},{20,24},{24,28},{28,32},{32,36}... | collective-permute-start | bytes 3080 | tf_op jit(solution)/shard_map/ppermute | solution.py:25
  248.9 8.3 %slice-start = ((s8[6291456]{0:T(1024)(128)(4,1)}), s8[2097152]{0:T(1024)(128)(4,1)S(1)}, s32[]{:S(2)}) async-start(s8[6291456]{0:T(1024)(128)(4,1)} %bitcast.36), calls=%async_computation.5 | async-start | bytes 4194304
  253.5 3.7 %slice-start.1 = ((s8[6291456]{0:T(1024)(128)(4,1)}), s8[4194304]{0:T(1024)(128)(4,1)S(1)}, s32[]{:S(2)}) async-start(s8[6291456]{0:T(1024)(128)(4,1)} %bitcast.36), calls=%async_computation.6 | async-start | bytes 8388608
  258.2 5.3 %copy-start = (f32[8,256,512]{2,1,0:T(8,128)}, f32[8,256,512]{2,1,0:T(8,128)S(1)}, u32[]{:S(2)}) copy-start(f32[8,256,512]{2,1,0:T(8,128)S(1)} %fusion.1) | copy-start | bytes 12582916
  297.9 18.8 %all-to-all-start = ((bf16[4,256,512]{1,2,0:T(8,128)(2,1)}), bf16[4,256,512]{1,2,0:T(8,128)(2,1)S(1)}, u32[]{:S(2)}, u32[]{:S(2)}) async-start(bf16[4,256,512]{1,2,0:T(8,128)(2,1)} %broadcast_in_dim.45), calls=%async_computation | async-start | bytes 2097152 | tf_op jit(solution)/shard_map/all_to_all | solution.py:45
Sparse Core Ops, SparseCore 0:
  39.2 209.6 all-gather.1
